TPU v7x, 32 devices: a whole 2x2x4 slice. The times are simulated.
32 devices in a mesh: sp: 4 (over y, x), dp: 8 (over z, core).
Axes of the slice: x: 2, y: 2, z: 4, core: 2. Of those that a mesh axis runs over, the one named last changes fastest.
Arguments:
- value_half: bfloat16 [8, 1024, 2048], P('dp', 'sp'), may hold values from -6 to 6
- gate_half: bfloat16 [8, 1024, 2048], P('dp', 'sp'), may hold values from -6 to 6
- upstream: bfloat16 [8, 1024, 2048], P('dp', 'sp'), may hold values from -6 to 6
- conv_taps: float32 [31, 2048], P(None, 'sp'), may hold values from -1 to 1
- norm_gain: float32 [2048], replicated, may hold values from 0.1 to 1.9
- out_weight: bfloat16 [2048, 2048], P('dp'), may hold values from -0.125 to 0.125
Outputs:
- grad_value: bfloat16 [8, 1024, 2048], P('dp', 'sp')
- grad_gate: bfloat16 [8, 1024, 2048], P('dp', 'sp')
- grad_taps: float32 [31, 2048], P(None, 'sp')
- grad_gain: float32 [2048], replicated
- grad_weight: float32 [2048, 2048], P('dp')
All inputs are finite; a program needn't handle non-finite values.
Results may differ from a plain program's by a relative error of at most 0.0062.
Values may be sent and summed in bfloat16 or wider, within the bound.
A program may use at most 128 MiB of HBM per device.

v0:
```python
import jax
import jax.numpy as jnp
from jax import lax
from jax.sharding import PartitionSpec as P

NORM_EPS = 1e-05


def body(value_half, gate_half, upstream, conv_taps, norm_gain, out_weight):
    tap_count = conv_taps.shape[0]
    sig_gate = jax.nn.sigmoid(gate_half.astype(jnp.float32))
    value_wide = value_half.astype(jnp.float32)
    glu = (value_wide * sig_gate).astype(jnp.bfloat16)
    glu_heads = lax.all_to_all(glu, "sp", split_axis=2, concat_axis=1, tiled=True).astype(
        jnp.float32
    )
    length = glu_heads.shape[1]
    padded = jnp.pad(glu_heads, ((0, 0), (tap_count - 1, 0), (0, 0)))
    conv_out = jnp.zeros_like(glu_heads)
    for offset in range(tap_count):
        conv_out = conv_out + conv_taps[offset] * padded[:, offset : offset + length]
    conv_tokens = lax.all_to_all(
        conv_out.astype(jnp.bfloat16), "sp", split_axis=1, concat_axis=2, tiled=True
    ).astype(jnp.float32)
    row_mean = jnp.mean(conv_tokens, axis=-1, keepdims=True)
    centered = conv_tokens - row_mean
    inv_scale = lax.rsqrt(jnp.mean(centered * centered, axis=-1, keepdims=True) + NORM_EPS)
    normed = centered * inv_scale
    scaled = normed * norm_gain
    sig_scaled = jax.nn.sigmoid(scaled)
    activated = (scaled * sig_scaled).astype(jnp.bfloat16)[0]
    upstream_rows = upstream[0]
    columns = upstream_rows
    grad_act = jnp.dot(
        columns,
        lax.all_gather(out_weight, "dp", axis=0, tiled=True),
        preferred_element_type=jnp.float32,
    )
    grad_scaled = grad_act[None] * sig_scaled * (1.0 + scaled * (1.0 - sig_scaled))
    gain_part = jnp.sum(grad_scaled * normed, axis=(0, 1))
    grad_normed = grad_scaled * norm_gain
    grad_conv_out = inv_scale * (
        grad_normed
        - jnp.mean(grad_normed, axis=-1, keepdims=True)
        - normed * jnp.mean(grad_normed * normed, axis=-1, keepdims=True)
    )
    grad_heads = lax.all_to_all(
        grad_conv_out.astype(jnp.bfloat16), "sp", split_axis=2, concat_axis=1, tiled=True
    ).astype(jnp.float32)
    grad_padded = jnp.pad(grad_heads, ((0, 0), (0, tap_count - 1), (0, 0)))
    grad_glu = jnp.zeros_like(grad_heads)
    tap_terms = []
    for offset in range(tap_count):
        first = tap_count - 1 - offset
        grad_glu = grad_glu + conv_taps[offset] * grad_padded[:, first : first + length]
        tap_terms.append(jnp.sum(grad_heads * padded[:, offset : offset + length], axis=(0, 1)))
    grad_taps = lax.psum(jnp.stack(tap_terms), "dp")
    grad_tokens = lax.all_to_all(
        grad_glu.astype(jnp.bfloat16), "sp", split_axis=1, concat_axis=2, tiled=True
    ).astype(jnp.float32)
    grad_value = (grad_tokens * sig_gate).astype(jnp.bfloat16)
    grad_gate = (grad_tokens * value_wide * sig_gate * (1.0 - sig_gate)).astype(jnp.bfloat16)
    grad_gain = lax.psum(gain_part, ("sp", "dp"))
    columns = upstream_rows
    owned = lax.psum_scatter(
        lax.dot_general(
            columns, activated, (((0,), (0,)), ((), ())), preferred_element_type=jnp.float32
        ),
        "dp",
        scatter_dimension=0,
        tiled=True,
    )
    grad_weight = lax.psum(owned, "sp")
    return (grad_value, grad_gate, grad_taps, grad_gain, grad_weight)


def solution(mesh):
    placed = (
        P("dp", "sp", None),
        P("dp", "sp", None),
        P("dp", "sp", None),
        P(None, "sp"),
        P(),
        P("dp", None),
    )
    return jax.shard_map(
        body,
        mesh=mesh,
        in_specs=placed,
        out_specs=(P("dp", "sp", None), P("dp", "sp", None), P(None, "sp"), P(), P("dp", None)),
        check_vma=False,
    )
```

profile of v0, /device:TPU:0, one launch (start us, length us, event | category | flops | bytes accessed | tf_op | source)
XLA Modules:
  0.0 395.5 jit_solution(13518251392995277205)
XLA Ops:
  11.9 12.9 %copy.90 = bf16[1,256,2048]{1,0,2:T(2,128)(2,1)} copy(bf16[1,256,2048]{1,2,0:T(8,128)(2,1)S(1)} %fusion.1) | data formatting | bytes 2097152 | tf_op jit(solution)/shard_map/convert_element_type | solution.py:13
  25.3 11.6 %reduce.17 = bf16[2048,256]{1,0:T(8,128)(2,1)S(1)} reduce(bf16[2048,1,256]{2,1,0:T(2,128)(2,1)} %bitcast.178, bf16[]{:T(256)} %broadcast.201), dimensions={1}, to_apply=%bitcast.161.reduce_sub_computation | reduce | bytes 2097154
  38.6 5.4 %all-to-all-start = ((bf16[4,2,65536]{2,1,0:T(2,128)(2,1)}), bf16[4,2,65536]{2,1,0:T(2,128)(2,1)}, u32[]{:S(2)}, u32[]{:S(2)}) async-start(bf16[4,2,65536]{2,1,0:T(2,128)(2,1)} %reshape.389), calls=%async_computation | async-start | bytes 2097152 | tf_op jit(solution)/shard_map/all_to_all | solution.py:14
  44.1 14.2 %all-to-all-done = bf16[4,2,65536]{2,1,0:T(2,128)(2,1)} async-done(((bf16[4,2,65536]{2,1,0:T(2,128)(2,1)}), bf16[4,2,65536]{2,1,0:T(2,128)(2,1)}, u32[]{:S(2)}, u32[]{:S(2)}) %all-to-all-start) | async-done | bytes 1048608 | tf_op jit(solution)/shard_map/all_to_all | solution.py:14
  58.3 2.6 reshape.390
  64.9 8.0 %add_convert_fusion.1 = bf16[1,1024,512]{2,1,0:T(8,128)(2,1)S(1)} fusion(f32[1,1024,512]{2,1,0:T(8,128)S(1)} %bitcast.163, f32[512]{0:T(512)S(1)} %bitcast.207, f32[512]{0:T(512)S(1)} %bitcast.209, f32[512]{0:T(512)S(1)} %bitcast.213, f32[512]{0:T(512)S(1)} %bitcast.215, f32[512]{0:T(512)S(1)} %bitcast.217, f32[512]{0:T(512)S(1)} %bitcast.219, ...), kind=kLoop, calls=%fused_computation.88 | loop fusion | flops 32505856 | bytes 3209216 | tf_op jit(solution)/shard_map/convert_element_type | solution.py:23
  72.9 2.9 copy.89
  75.8 8.1 %reduce.18 = bf16[1024,512]{1,0:T(8,128)(2,1)S(1)} reduce(bf16[1024,1,512]{2,1,0:T(2,128)(2,1)} %bitcast.180, bf16[]{:T(256)} %broadcast.201), dimensions={1}, to_apply=%bitcast.160.reduce_sub_computation | reduce | bytes 2097154
  83.9 2.0 reshape.391
  85.9 4.3 %all-to-all-start.1 = ((bf16[4,2,65536]{2,1,0:T(2,128)(2,1)}), bf16[4,2,65536]{2,1,0:T(2,128)(2,1)}, u32[]{:S(2)}, u32[]{:S(2)}) async-start(bf16[4,2,65536]{2,1,0:T(2,128)(2,1)} %reshape.391), calls=%async_computation.1 | async-start | bytes 2097152 | tf_op jit(solution)/shard_map/all_to_all | solution.py:22
  90.2 13.4 %all-to-all-done.1 = bf16[4,2,65536]{2,1,0:T(2,128)(2,1)} async-done(((bf16[4,2,65536]{2,1,0:T(2,128)(2,1)}), bf16[4,2,65536]{2,1,0:T(2,128)(2,1)}, u32[]{:S(2)}, u32[]{:S(2)}) %all-to-all-start.1) | async-done | bytes 1048608 | tf_op jit(solution)/shard_map/all_to_all | solution.py:22
  103.6 3.0 reshape.392
  115.4 2.3 copy.71
  117.6 9.3 %convolution_bitcast_fusion = f32[2048,2048]{0,1:T(8,128)} fusion(bf16[256,2048]{0,1:T(8,128)(2,1)} %bitcast.186, bf16[1,256,2048]{2,1,0:T(8,128)(2,1)S(1)} %copy-done), kind=kOutput, calls=%fused_computation | convolution fusion | flops 2147483648 | bytes 18874368 | tf_op jit(solution)/shard_map/dot_general | solution.py:66
  129.2 5.7 %multiply_reduce_fusion = (f32[2048]{0:T(1024)S(1)}, f32[256]{0:T(256)S(1)}, f32[256]{0:T(256)S(1)}, f32[256,2048]{1,0:T(8,128)S(1)}) fusion(f32[256,2048]{1,0:T(8,128)S(1)} %bitcast.176, f32[256]{0:T(256)S(1)} %broadcast_multiply_fusion.2, f32[256]{0:T(256)S(1)} %add_rsqrt_fusion, f32[2048]{0:T(1024)S(1)} %copy-done.11, ...), kind=kOutput, calls=%fused_computation.20 | convolution fusion | flops 2156393984 | bytes 13651968 | tf_op jit(solution)/shard_map/dot_general | solution.py:34
  137.4 10.8 %reduce.19 = bf16[2048,256]{1,0:T(8,128)(2,1)S(1)} reduce(bf16[2048,1,256]{2,1,0:T(2,128)(2,1)S(1)} %bitcast.182, bf16[]{:T(256)} %broadcast.201), dimensions={1}, to_apply=%bitcast.148.reduce_sub_computation | reduce | bytes 2097154
  149.8 3.5 all-to-all-start.2
  153.4 48.8 %psum.22 = f32[2048]{0:T(1024)} all-reduce(f32[2048]{0:T(1024)S(1)} %get-tuple-element.35), channel_id=1, replica_groups=mesh['sp'=4,'dp'=8] {'sp','dp'}, use_global_device_ids=true, to_apply=%region_39.40 | all-reduce | flops 2048 | bytes 16384 | tf_op jit(solution)/shard_map/psum | solution.py:63
  207.1 8.0 %add_convert_fusion = bf16[1,1024,512]{2,1,0:T(8,128)(2,1)S(1)} fusion(f32[1,1024,512]{2,1,0:T(8,128)S(1)} %bitcast.162, f32[512]{0:T(512)S(1)} %bitcast.208, f32[512]{0:T(512)S(1)} %bitcast.210, f32[512]{0:T(512)S(1)} %bitcast.214, f32[512]{0:T(512)S(1)} %bitcast.216, f32[512]{0:T(512)S(1)} %bitcast.218, f32[512]{0:T(512)S(1)} %bitcast.220, ...), kind=kLoop, calls=%fused_computation.52 | loop fusion | flops 32505856 | bytes 3209216 | tf_op jit(solution)/shard_map/convert_element_type | solution.py:59
  215.0 81.4 %reduce-scatter.2.cloned.1.call-done = f32[256,2048]{0,1:T(8,128)} async-done(((f32[2048,2048]{0,1:T(8,128)}), f32[256,2048]{0,1:T(8,128)}) %reduce-scatter.2.cloned.1.call-update) | async-done | bytes 2097168 | tf_op jit(solution)/shard_map/reduce_scatter | solution.py:65
  296.5 17.9 %multiply_reduce_fusion.2 = (f32[512]{0:T(512)S(1)}, f32[512]{0:T(512)S(1)}, f32[512]{0:T(512)S(1)}, f32[512]{0:T(512)S(1)}, f32[512]{0:T(512)S(1)}, /*index=5*/...) fusion(f32[1,1024,512]{2,1,0:T(8,128)} %bitcast.164, ...), kind=kLoop, calls=%fused_computation.22 | loop fusion | flops 18865152 | bytes 4231168 | tf_op jit(solution)/shard_map/reduce_sum | solution.py:56
  314.4 2.9 copy.88
  317.4 8.0 %reduce.20 = bf16[1024,512]{1,0:T(8,128)(2,1)S(1)} reduce(bf16[1024,1,512]{2,1,0:T(2,128)(2,1)} %bitcast.179, bf16[]{:T(256)} %broadcast.201), dimensions={1}, to_apply=%bitcast.159.reduce_sub_computation | reduce | bytes 2097154
  325.4 2.0 reshape.395
  327.4 3.7 all-to-all-start.3
  331.1 2.6 multiply_reduce_fusion.1
  333.7 11.8 %multiply_reduce_fusion.3 = (f32[512]{0:T(512)S(1)}, f32[512]{0:T(512)S(1)}, f32[512]{0:T(512)S(1)}, f32[512]{0:T(512)S(1)}, f32[512]{0:T(512)S(1)}, /*index=5*/...) fusion(f32[1,1024,512]{2,1,0:T(8,128)} %bitcast.165, ...), kind=kLoop, calls=%fused_computation.23 | loop fusion | flops 12576768 | bytes 4218880 | tf_op jit(solution)/shard_map/reduce_sum | solution.py:56
  345.7 27.2 %psum.21 = f32[31,512]{1,0:T(8,128)} all-reduce(f32[31,512]{1,0:T(8,128)S(1)} %stack.127), channel_id=1, replica_groups=mesh['sp'=4,'dp'=8] {'dp'}, use_global_device_ids=true, to_apply=%region_37.38 | all-reduce | flops 15872 | bytes 126976 | tf_op jit(solution)/shard_map/psum | solution.py:57
  375.7 3.0 copy.70
  378.8 3.4 fusion.4
  382.1 2.3 copy.72
  385.8 2.9 copy.74
  (69 shorter events, 35.3 us)
Async XLA Ops:
  7.2 110.5 %copy-start = (bf16[1,256,2048]{2,1,0:T(8,128)(2,1)S(1)}, bf16[1,256,2048]{2,1,0:T(8,128)(2,1)}, u32[]{:S(2)}) copy-start(bf16[1,256,2048]{2,1,0:T(8,128)(2,1)} %param.8) | copy-start | bytes 3145732
  7.2 122.0 %all-gather.2.cloned.1.call-start = ((), (), s32[]{:S(2)}) async-start(), calls=%async_computation.5 | async-start | bytes 9437184 | tf_op jit(solution)/shard_map/all_gather | solution.py:36
  9.4 2.5 copy-start.6
  11.3 13.5 %copy-start.8 = (bf16[1,256,2048]{1,2,0:T(8,128)(2,1)}, bf16[1,256,2048]{1,2,0:T(8,128)(2,1)S(1)}, u32[]{:S(2)}) copy-start(bf16[1,256,2048]{1,2,0:T(8,128)(2,1)S(1)} %copy.57) | copy-start | bytes 3145732
  37.0 7.1 %copy-start.10 = (f32[31,512]{1,0:T(8,128)S(1)}, f32[31,512]{1,0:T(8,128)}, u32[]{:S(2)}) copy-start(f32[31,512]{1,0:T(8,128)} %param.9) | copy-start | bytes 190468
  38.6 19.7 %all-to-all-start = ((bf16[4,2,65536]{2,1,0:T(2,128)(2,1)}), bf16[4,2,65536]{2,1,0:T(2,128)(2,1)}, u32[]{:S(2)}, u32[]{:S(2)}) async-start(bf16[4,2,65536]{2,1,0:T(2,128)(2,1)} %reshape.389), calls=%async_computation | async-start | bytes 2097152 | tf_op jit(solution)/shard_map/all_to_all | solution.py:14
  60.9 2.0 copy-start.3
  64.9 10.9 %copy-start.2 = (f32[1,4,256,512]{3,2,1,0:T(8,128)}, f32[1,4,256,512]{3,2,1,0:T(8,128)S(1)}, u32[]{:S(2)}) copy-start(f32[1,4,256,512]{3,2,1,0:T(8,128)S(1)} %copy.60) | copy-start | bytes 6291460
  83.9 6.3 %copy-start.11 = (f32[2048]{0:T(1024)S(1)}, f32[2048]{0:T(1024)}, u32[]{:S(2)}) copy-start(f32[2048]{0:T(1024)} %param.10) | copy-start | bytes 24580
  85.9 17.7 %all-to-all-start.1 = ((bf16[4,2,65536]{2,1,0:T(2,128)(2,1)}), bf16[4,2,65536]{2,1,0:T(2,128)(2,1)}, u32[]{:S(2)}, u32[]{:S(2)}) async-start(bf16[4,2,65536]{2,1,0:T(2,128)(2,1)} %reshape.391), calls=%async_computation.1 | async-start | bytes 2097152 | tf_op jit(solution)/shard_map/all_to_all | solution.py:22
  90.2 206.3 %reduce-scatter.2.cloned.1.call-start = ((), (), s32[]{:S(2)}) async-start(), calls=%async_computation.6 | async-start | bytes 18874368 | tf_op jit(solution)/shard_map/reduce_scatter | solution.py:65
  106.6 1.3 copy-start.5
  149.8 52.3 %all-to-all-start.2 = ((bf16[4,2,65536]{2,1,0:T(2,128)(2,1)}), bf16[4,2,65536]{2,1,0:T(2,128)(2,1)S(1)}, u32[]{:S(2)}, u32[]{:S(2)}) async-start(bf16[4,2,65536]{2,1,0:T(2,128)(2,1)} %reshape.393), calls=%async_computation.2 | async-start | bytes 2097152 | tf_op jit(solution)/shard_map/all_to_all | solution.py:47
  153.3 232.5 %all-reduce.4.cloned.1.call-start = ((), (), s32[]{:S(2)}) async-start(), calls=%async_computation.7 | async-start | bytes 4194304 | tf_op jit(solution)/shard_map/psum | solution.py:73
  203.1 2.0 copy-start.4
  327.4 45.5 %all-to-all-start.3 = ((bf16[4,2,65536]{2,1,0:T(2,128)(2,1)}), bf16[4,2,65536]{2,1,0:T(2,128)(2,1)S(1)}, u32[]{:S(2)}, u32[]{:S(2)}) async-start(bf16[4,2,65536]{2,1,0:T(2,128)(2,1)} %reshape.395), calls=%async_computation.3 | async-start | bytes 2097152 | tf_op jit(solution)/shard_map/all_to_all | solution.py:58
  375.7 3.0 copy-start.7
  375.7 3.0 copy-start.9
  384.4 4.3 %copy-start.1 = (bf16[1,256,2048]{2,1,0:T(8,128)(2,1)S(1)}, bf16[1,256,2048]{2,1,0:T(8,128)(2,1)}, u32[]{:S(2)}) copy-start(bf16[1,256,2048]{2,1,0:T(8,128)(2,1)} %param.8) | copy-start | bytes 3145732
Sparse Core Ops, SparseCore 0:
  9.6 84.7 all-gather.1
  127.1 169.3 reduce-scatter.1
  299.6 69.1 all-reduce.3
where the time goes:
time: 402 us; the launch traced here: 395 us
  waiting for transfers between devices  110 us (27%)
  other arithmetic  102 us (25%)
  blocking collectives  75.9 us (19%)
  local copies, waits for them, and re-layouts  61.5 us (15%)
  starting transfers between devices  16.9 us (4%)
  matrix products  15 us (4%)
  between operations  14.3 us (4%)
    reduce_scatter x1, waiting for transfers between devices, body(): lax.psum_scatter(lax.dot_general(columns, activated, (((0,), (0,)), ((),...  81.4 us
    psum x1, blocking collectives, body(): grad_gain = lax.psum(gain_part, ('sp', 'dp'))  48.8 us
    unnamed x4, other arithmetic  38.5 us
    reduce_sum x4, other arithmetic, body(): jnp.sum(grad_heads * padded[:, offset:offset + length], axis=(0, 1))  32.4 us
    unnamed x39, local copies, waits for them, and re-layouts  28.2 us
    psum x1, blocking collectives, body(): grad_taps = lax.psum(jnp.stack(tap_terms), 'dp')  27.2 us
    all_to_all x1, waiting for transfers between devices, body(): lax.all_to_all(glu, 'sp', split_axis=2, concat_axis=1, tiled=True)  14.2 us
    all_to_all x1, waiting for transfers between devices, body(): lax.all_to_all(conv_out.astype(jnp.bfloat16), 'sp', split_axis=1, concat_...  13.4 us
  transfers between devices with their start and end apart: 7, of which 3 were waited for; matrix products, arithmetic and copies ran while one was open for 44% of the time, Pallas kernels for 0%

commit v1 on v0

--- a/solution.py
+++ b/solution.py
@@ -60,7 +60,7 @@
     ).astype(jnp.float32)
     grad_value = (grad_tokens * sig_gate).astype(jnp.bfloat16)
     grad_gate = (grad_tokens * value_wide * sig_gate * (1.0 - sig_gate)).astype(jnp.bfloat16)
-    grad_gain = lax.psum(gain_part, ("sp", "dp"))
+    grad_gain = lax.psum(lax.psum(gain_part, "sp"), "dp")
     columns = upstream_rows
     owned = lax.psum_scatter(
         lax.dot_general(

time: 402 us -> 443 us (1.10)
  waiting for transfers between devices: 110 us -> 206 us
  blocking collectives: 75.9 us -> 17 us
  local copies, waits for them, and re-layouts: 61.5 us -> 66.5 us
    psum x2 -> x1, blocking collectives: 75.9 us -> 17 us  [body(): grad_gain = lax.psum(lax.psum(gain_part, 'sp'), 'dp')]
    psum x0 -> x1, waiting for transfers between devices: none -> 50.3 us  [body(): grad_taps = lax.psum(jnp.stack(tap_terms), 'dp')]
    reduce_scatter x1, waiting for transfers between devices: 81.4 us -> 120 us  [body(): lax.psum_scatter(lax.dot_general(columns, activated, (((0,), (0,)), ((),...]
    psum x1, waiting for transfers between devices: 0.01 us -> 7.13 us  [body(): grad_weight = lax.psum(owned, 'sp')]
    unnamed x39 -> x45, local copies, waits for them, and re-layouts: 28.2 us -> 30.8 us
  transfers between devices with their start and end apart: 7 -> 8, of which waited for: 3 -> 5; matrix products, arithmetic and copies ran while one was open for 44% -> 41% of each run, Pallas kernels for 0% -> 0%
where the time goes in v1:
time: 443 us; the launch traced here: 436 us
  waiting for transfers between devices  206 us (47%)
  other arithmetic  100 us (23%)
  local copies, waits for them, and re-layouts  66.5 us (15%)
  starting transfers between devices  17 us (4%)
  blocking collectives  17 us (4%)
  matrix products  15 us (3%)
  between operations  14.3 us (3%)
    reduce_scatter x1, waiting for transfers between devices, body(): lax.psum_scatter(lax.dot_general(columns, activated, (((0,), (0,)), ((),...  120 us
    psum x1, waiting for transfers between devices, body(): grad_taps = lax.psum(jnp.stack(tap_terms), 'dp')  50.3 us
    unnamed x4, other arithmetic  38.8 us
    unnamed x45, local copies, waits for them, and re-layouts  30.8 us
    reduce_sum x4, other arithmetic, body(): jnp.sum(grad_heads * padded[:, offset:offset + length], axis=(0, 1))  30.3 us
    psum x1, blocking collectives, body(): grad_gain = lax.psum(lax.psum(gain_part, 'sp'), 'dp')  17 us
    all_to_all x1, waiting for transfers between devices, body(): lax.all_to_all(glu, 'sp', split_axis=2, concat_axis=1, tiled=True)  14.2 us
    all_to_all x1, waiting for transfers between devices, body(): lax.all_to_all(conv_out.astype(jnp.bfloat16), 'sp', split_axis=1, concat_...  13.4 us
  transfers between devices with their start and end apart: 8, of which 5 were waited for; matrix products, arithmetic and copies ran while one was open for 41% of the time, Pallas kernels for 0%

profile of v1, /device:TPU:0, one launch (start us, length us, event | category | flops | bytes accessed | tf_op | source)
XLA Modules:
  0.0 435.8 jit_solution(4021218117244527981)
XLA Ops:
  11.9 12.9 %copy.90 = bf16[1,256,2048]{1,0,2:T(2,128)(2,1)} copy(bf16[1,256,2048]{1,2,0:T(8,128)(2,1)S(1)} %fusion.1) | data formatting | bytes 2097152 | tf_op jit(solution)/shard_map/convert_element_type | solution.py:13
  25.3 11.6 %reduce.17 = bf16[2048,256]{1,0:T(8,128)(2,1)S(1)} reduce(bf16[2048,1,256]{2,1,0:T(2,128)(2,1)} %bitcast.178, bf16[]{:T(256)} %broadcast.201), dimensions={1}, to_apply=%bitcast.161.reduce_sub_computation | reduce | bytes 2097154
  38.6 5.4 %all-to-all-start = ((bf16[4,2,65536]{2,1,0:T(2,128)(2,1)}), bf16[4,2,65536]{2,1,0:T(2,128)(2,1)}, u32[]{:S(2)}, u32[]{:S(2)}) async-start(bf16[4,2,65536]{2,1,0:T(2,128)(2,1)} %reshape.389), calls=%async_computation | async-start | bytes 2097152 | tf_op jit(solution)/shard_map/all_to_all | solution.py:14
  44.1 14.2 %all-to-all-done = bf16[4,2,65536]{2,1,0:T(2,128)(2,1)} async-done(((bf16[4,2,65536]{2,1,0:T(2,128)(2,1)}), bf16[4,2,65536]{2,1,0:T(2,128)(2,1)}, u32[]{:S(2)}, u32[]{:S(2)}) %all-to-all-start) | async-done | bytes 1048608 | tf_op jit(solution)/shard_map/all_to_all | solution.py:14
  58.3 2.6 reshape.390
  64.9 8.0 %add_convert_fusion.1 = bf16[1,1024,512]{2,1,0:T(8,128)(2,1)S(1)} fusion(f32[1,1024,512]{2,1,0:T(8,128)S(1)} %bitcast.163, f32[512]{0:T(512)S(1)} %bitcast.207, f32[512]{0:T(512)S(1)} %bitcast.209, f32[512]{0:T(512)S(1)} %bitcast.213, f32[512]{0:T(512)S(1)} %bitcast.215, f32[512]{0:T(512)S(1)} %bitcast.217, f32[512]{0:T(512)S(1)} %bitcast.219, ...), kind=kLoop, calls=%fused_computation.88 | loop fusion | flops 32505856 | bytes 3209216 | tf_op jit(solution)/shard_map/convert_element_type | solution.py:23
  72.9 2.9 copy.89
  75.8 8.1 %reduce.18 = bf16[1024,512]{1,0:T(8,128)(2,1)S(1)} reduce(bf16[1024,1,512]{2,1,0:T(2,128)(2,1)} %bitcast.180, bf16[]{:T(256)} %broadcast.201), dimensions={1}, to_apply=%bitcast.160.reduce_sub_computation | reduce | bytes 2097154
  83.9 2.0 reshape.391
  85.9 4.3 all-to-all-start.1
  90.2 13.4 %all-to-all-done.1 = bf16[4,2,65536]{2,1,0:T(2,128)(2,1)} async-done(((bf16[4,2,65536]{2,1,0:T(2,128)(2,1)}), bf16[4,2,65536]{2,1,0:T(2,128)(2,1)}, u32[]{:S(2)}, u32[]{:S(2)}) %all-to-all-start.1) | async-done | bytes 1048608 | tf_op jit(solution)/shard_map/all_to_all | solution.py:22
  103.6 2.8 reshape.392
  115.2 2.3 copy.71
  117.4 9.3 %convolution_bitcast_fusion = f32[2048,2048]{0,1:T(8,128)} fusion(bf16[256,2048]{0,1:T(8,128)(2,1)} %bitcast.186, bf16[1,256,2048]{2,1,0:T(8,128)(2,1)S(1)} %copy-done), kind=kOutput, calls=%fused_computation | convolution fusion | flops 2147483648 | bytes 18874368 | tf_op jit(solution)/shard_map/dot_general | solution.py:66
  129.0 5.8 %multiply_reduce_fusion = (f32[2048]{0:T(1024)S(1)}, f32[256]{0:T(256)S(1)}, f32[256]{0:T(256)S(1)}, f32[256,2048]{1,0:T(8,128)S(1)}) fusion(f32[256,2048]{1,0:T(8,128)S(1)} %bitcast.176, f32[256]{0:T(256)S(1)} %broadcast_multiply_fusion.2, f32[256]{0:T(256)S(1)} %add_rsqrt_fusion, f32[2048]{0:T(1024)S(1)} %copy-done.13, ...), kind=kOutput, calls=%fused_computation.20 | convolution fusion | flops 2156393984 | bytes 13651968 | tf_op jit(solution)/shard_map/dot_general | solution.py:34
  137.2 11.0 %reduce.19 = bf16[2048,256]{1,0:T(8,128)(2,1)S(1)} reduce(bf16[2048,1,256]{2,1,0:T(2,128)(2,1)S(1)} %bitcast.182, bf16[]{:T(256)} %broadcast.201), dimensions={1}, to_apply=%bitcast.148.reduce_sub_computation | reduce | bytes 2097154
  149.8 3.5 all-to-all-start.2
  153.4 17.0 %psum.29 = f32[2048]{0:T(1024)} all-reduce(f32[2048]{0:T(1024)S(1)} %get-tuple-element.35), channel_id=1, replica_groups=mesh['sp'=4,'dp'=8] {'sp'}, use_global_device_ids=true, to_apply=%region_39.40 | all-reduce | flops 2048 | bytes 16384 | tf_op jit(solution)/shard_map/psum | solution.py:63
  175.3 119.9 %reduce-scatter.2.cloned.1.call-done = f32[256,2048]{0,1:T(8,128)} async-done(((f32[2048,2048]{0,1:T(8,128)}), f32[256,2048]{0,1:T(8,128)}) %reduce-scatter.2.cloned.1.call-update) | async-done | bytes 2097168 | tf_op jit(solution)/shard_map/reduce_scatter | solution.py:65
  295.3 8.0 %add_convert_fusion = bf16[1,1024,512]{2,1,0:T(8,128)(2,1)S(1)} fusion(f32[1,1024,512]{2,1,0:T(8,128)S(1)} %bitcast.162, f32[512]{0:T(512)S(1)} %bitcast.208, f32[512]{0:T(512)S(1)} %bitcast.210, f32[512]{0:T(512)S(1)} %bitcast.214, f32[512]{0:T(512)S(1)} %bitcast.216, f32[512]{0:T(512)S(1)} %bitcast.218, f32[512]{0:T(512)S(1)} %bitcast.220, ...), kind=kLoop, calls=%fused_computation.52 | loop fusion | flops 32505856 | bytes 3209216 | tf_op jit(solution)/shard_map/convert_element_type | solution.py:59
  303.2 2.9 copy.88
  306.2 8.0 %reduce.20 = bf16[1024,512]{1,0:T(8,128)(2,1)S(1)} reduce(bf16[1024,1,512]{2,1,0:T(2,128)(2,1)} %bitcast.179, bf16[]{:T(256)} %broadcast.201), dimensions={1}, to_apply=%bitcast.159.reduce_sub_computation | reduce | bytes 2097154
  316.2 3.7 all-to-all-start.3
  319.9 18.1 %multiply_reduce_fusion.2 = (f32[512]{0:T(512)S(1)}, f32[512]{0:T(512)S(1)}, f32[512]{0:T(512)S(1)}, f32[512]{0:T(512)S(1)}, f32[512]{0:T(512)S(1)}, /*index=5*/...) fusion(f32[1,1024,512]{2,1,0:T(8,128)} %bitcast.164, ...), kind=kLoop, calls=%fused_computation.22 | loop fusion | flops 18865152 | bytes 4231168 | tf_op jit(solution)/shard_map/reduce_sum | solution.py:56
  338.4 11.8 %multiply_reduce_fusion.3 = (f32[512]{0:T(512)S(1)}, f32[512]{0:T(512)S(1)}, f32[512]{0:T(512)S(1)}, f32[512]{0:T(512)S(1)}, f32[512]{0:T(512)S(1)}, /*index=5*/...) fusion(f32[1,1024,512]{2,1,0:T(8,128)} %bitcast.165, ...), kind=kLoop, calls=%fused_computation.23 | loop fusion | flops 12576768 | bytes 4218880 | tf_op jit(solution)/shard_map/reduce_sum | solution.py:56
  350.3 2.5 stack.127
  355.7 3.0 copy.70
  358.8 3.6 fusion.4
  362.4 2.3 copy.72
  366.1 7.1 %all-reduce.6.cloned.1.call-done = f32[256,2048]{0,1:T(8,128)} async-done(((f32[256,2048]{0,1:T(8,128)}), f32[256,2048]{0,1:T(8,128)}) %all-reduce.6.cloned.1.call-update) | async-done | bytes 2097168 | tf_op jit(solution)/shard_map/psum | solution.py:73
  373.2 2.9 copy.74
  376.1 50.3 %all-reduce.8.cloned.1.call-done = (f32[31,512]{1,0:T(8,128)}, f32[2048]{0:T(1024)}) async-done(((f32[31,512]{1,0:T(8,128)}, f32[2048]{0:T(1024)}), (f32[31,512]{1,0:T(8,128)}, f32[2048]{0:T(1024)})) %all-reduce.8.cloned.1.call-update) | async-done | bytes 71696 | tf_op jit(solution)/shard_map/psum | solution.py:57
  (77 shorter events, 40.3 us)
Async XLA Ops:
  7.2 110.3 %copy-start = (bf16[1,256,2048]{2,1,0:T(8,128)(2,1)S(1)}, bf16[1,256,2048]{2,1,0:T(8,128)(2,1)}, u32[]{:S(2)}) copy-start(bf16[1,256,2048]{2,1,0:T(8,128)(2,1)} %param.8) | copy-start | bytes 3145732
  7.2 121.8 %all-gather.2.cloned.1.call-start = ((), (), s32[]{:S(2)}) async-start(), calls=%async_computation.5 | async-start | bytes 9437184 | tf_op jit(solution)/shard_map/all_gather | solution.py:36
  9.4 2.5 copy-start.8
  11.3 13.5 %copy-start.10 = (bf16[1,256,2048]{1,2,0:T(8,128)(2,1)}, bf16[1,256,2048]{1,2,0:T(8,128)(2,1)S(1)}, u32[]{:S(2)}) copy-start(bf16[1,256,2048]{1,2,0:T(8,128)(2,1)S(1)} %copy.57) | copy-start | bytes 3145732
  37.0 7.0 %copy-start.12 = (f32[31,512]{1,0:T(8,128)S(1)}, f32[31,512]{1,0:T(8,128)}, u32[]{:S(2)}) copy-start(f32[31,512]{1,0:T(8,128)} %param.9) | copy-start | bytes 190468
  38.6 19.7 %all-to-all-start = ((bf16[4,2,65536]{2,1,0:T(2,128)(2,1)}), bf16[4,2,65536]{2,1,0:T(2,128)(2,1)}, u32[]{:S(2)}, u32[]{:S(2)}) async-start(bf16[4,2,65536]{2,1,0:T(2,128)(2,1)} %reshape.389), calls=%async_computation | async-start | bytes 2097152 | tf_op jit(solution)/shard_map/all_to_all | solution.py:14
  60.9 2.0 copy-start.3
  64.9 10.9 %copy-start.2 = (f32[1,4,256,512]{3,2,1,0:T(8,128)}, f32[1,4,256,512]{3,2,1,0:T(8,128)S(1)}, u32[]{:S(2)}) copy-start(f32[1,4,256,512]{3,2,1,0:T(8,128)S(1)} %copy.60) | copy-start | bytes 6291460
  83.9 6.3 %copy-start.13 = (f32[2048]{0:T(1024)S(1)}, f32[2048]{0:T(1024)}, u32[]{:S(2)}) copy-start(f32[2048]{0:T(1024)} %param.10) | copy-start | bytes 24580
  85.9 17.7 %all-to-all-start.1 = ((bf16[4,2,65536]{2,1,0:T(2,128)(2,1)}), bf16[4,2,65536]{2,1,0:T(2,128)(2,1)}, u32[]{:S(2)}, u32[]{:S(2)}) async-start(bf16[4,2,65536]{2,1,0:T(2,128)(2,1)} %reshape.391), calls=%async_computation.1 | async-start | bytes 2097152 | tf_op jit(solution)/shard_map/all_to_all | solution.py:22
  90.2 205.1 %reduce-scatter.2.cloned.1.call-start = ((), (), s32[]{:S(2)}) async-start(), calls=%async_computation.6 | async-start | bytes 18874368 | tf_op jit(solution)/shard_map/reduce_scatter | solution.py:65
  106.4 1.3 copy-start.7
  149.8 20.6 %all-to-all-start.2 = ((bf16[4,2,65536]{2,1,0:T(2,128)(2,1)}), bf16[4,2,65536]{2,1,0:T(2,128)(2,1)S(1)}, u32[]{:S(2)}, u32[]{:S(2)}) async-start(bf16[4,2,65536]{2,1,0:T(2,128)(2,1)} %reshape.393), calls=%async_computation.2 | async-start | bytes 2097152 | tf_op jit(solution)/shard_map/all_to_all | solution.py:47
  153.4 219.8 %all-reduce.6.cloned.1.call-start = ((), (), s32[]{:S(2)}) async-start(), calls=%async_computation.7 | async-start | bytes 4194304 | tf_op jit(solution)/shard_map/psum | solution.py:73
  171.4 2.0 copy-start.5
  316.2 36.6 %all-to-all-start.3 = ((bf16[4,2,65536]{2,1,0:T(2,128)(2,1)}), bf16[4,2,65536]{2,1,0:T(2,128)(2,1)S(1)}, u32[]{:S(2)}, u32[]{:S(2)}) async-start(bf16[4,2,65536]{2,1,0:T(2,128)(2,1)} %reshape.395), calls=%async_computation.3 | async-start | bytes 2097152 | tf_op jit(solution)/shard_map/all_to_all | solution.py:58
  319.9 106.4 %all-reduce.8.cloned.1.call-start = ((), (), s32[]{:S(2)}) async-start(), calls=%async_computation.8 | async-start | bytes 147456 | tf_op jit(solution)/shard_map/psum | solution.py:57
  319.9 18.1 %copy-start.4 = (bf16[2048,1,256]{2,1,0:T(2,128)(2,1)S(1)}, bf16[2048,1,256]{2,1,0:T(2,128)(2,1)}, u32[]{:S(2)}) copy-start(bf16[2048,1,256]{2,1,0:T(2,128)(2,1)} %copy-done.3) | copy-start | bytes 3145732
  319.9 18.1 %copy-start.6 = (bf16[2048,1,256]{2,1,0:T(2,128)(2,1)S(1)}, bf16[2048,1,256]{2,1,0:T(2,128)(2,1)}, u32[]{:S(2)}) copy-start(bf16[2048,1,256]{2,1,0:T(2,128)(2,1)} %copy-done.5) | copy-start | bytes 3145732
  355.7 3.0 copy-start.9
  355.7 3.0 copy-start.11
  364.7 64.5 %copy-start.1 = (bf16[1,256,2048]{2,1,0:T(8,128)(2,1)S(1)}, bf16[1,256,2048]{2,1,0:T(8,128)(2,1)}, u32[]{:S(2)}) copy-start(bf16[1,256,2048]{2,1,0:T(8,128)(2,1)} %param.8) | copy-start | bytes 3145732
Sparse Core Ops, SparseCore 0:
  9.6 84.7 all-gather.1
  126.9 168.3 reduce-scatter.1
  298.4 74.7 all-reduce.5
  376.0 50.2 all-reduce.7
